TPU v7x, 32 devices: a whole 2x2x4 slice. The times are simulated.
32 devices in a mesh: ep: 8 (over z, core), tp: 4 (over y, x).
Axes of the slice: x: 2, y: 2, z: 4, core: 2. Of those that a mesh axis runs over, the one named last changes fastest.
Arguments:
- branch_in: bfloat16 [8192, 512], P(('ep', 'tp')), may hold values from -6 to 6
- pool_weight: bfloat16 [4, 128, 128], replicated, may hold values from -0.5 to 0.5
- group_gain: float32 [512], replicated, may hold values from 0.1 to 1.9
- out_weight: bfloat16 [512, 2048], P(None, 'tp'), may hold values from -0.25 to 0.25
- out_gain: float32 [2048], replicated, may hold values from 0.1 to 1.9
- ffn_input: bfloat16 [1024, 2048], P('ep'), may hold values from -6 to 6
- ffn_gain: float32 [2048], replicated, may hold values from 0.1 to 1.9
- routes: int32 [1024, 4], P('ep'), may hold values from 0 to 7, all different within a row; in each aligned block of 128 rows (0 to 127, 128 to 255, ...) at most 128 rows name the same one
- route_weight: float32 [1024, 4], P('ep'), may hold values from 0.2 to 2
- gate_weight: bfloat16 [8, 2048, 4096], P('ep', None, 'tp'), may hold values from -0.375 to 0.375
- up_weight: bfloat16 [8, 2048, 4096], P('ep', None, 'tp'), may hold values from -0.375 to 0.375
- down_weight: bfloat16 [8, 4096, 2048], P('ep', 'tp'), may hold values from -0.0078125 to 0.0078125
Outputs:
- mixer_out: bfloat16 [8192, 2048], P(('ep', 'tp'))
- expert_out: bfloat16 [1024, 2048], P('ep', 'tp')
Inputs may be any that keep to these rules, and one draw needn't show every extreme that they name: `routes`: each row names 4 different experts. Among the 128 rows of one index of ep no expert is named by more than 128 rows, and in some such block one expert is named by exactly 128.
All inputs are finite; a program needn't handle non-finite values.
Results may differ from a plain program's by a relative error of at most 0.017.
Values may be sent and summed in bfloat16 or wider, within the bound.
A program may use at most 64 MiB of HBM per device.

v0:
```python
import jax
import jax.numpy as jnp
from jax import lax
from jax.sharding import PartitionSpec as P

pool_windows = (2, 4, 8, 16)
rim_rows = 15
norm_eps = 1e-06
clamp_limit = 7.0
sigmoid_slope = 1.702


def shifted_2(block, axis, distance):
    devices = range(lax.axis_size(axis))
    route = [(i - distance, i) for i in devices if i - distance in devices]
    return lax.ppermute(block, axis, route)


def rms_scale(values, gain):
    return values * lax.rsqrt(jnp.mean(values * values, axis=-1, keepdims=True) + norm_eps) * gain


def slot_tables(route_block, expert_count, capacity):
    row_count, top_count = route_block.shape
    flat_experts = route_block.reshape(-1)
    one_hot = (flat_experts[:, None] == jnp.arange(expert_count, dtype=jnp.int32)[None, :]).astype(
        jnp.int32
    )
    earlier = jnp.cumsum(one_hot, axis=0) - one_hot
    slot_index = jnp.sum(earlier * one_hot, axis=1)
    flat_slots = slot_index * expert_count + flat_experts
    owner_rows = jnp.full((capacity * expert_count,), row_count, jnp.int32)
    owner_rows = owner_rows.at[flat_slots].set(
        jnp.arange(row_count * top_count, dtype=jnp.int32) // top_count
    )
    return (flat_slots, owner_rows)


def pool_branch(branch_in, pool_weight, group_gain, out_weight, out_gain):
    row_count, width = branch_in.shape
    group_chans = width // len(pool_windows)
    rim = shifted_2(branch_in[row_count - rim_rows :], ("ep", "tp"), 1)
    widened = jnp.concatenate([rim, branch_in], axis=0).astype(jnp.float32)
    first_row = (lax.axis_index("ep") * lax.axis_size("tp") + lax.axis_index("tp")) * row_count
    positions = first_row + jnp.arange(row_count, dtype=jnp.int32)
    window = jnp.repeat(jnp.array(pool_windows, jnp.int32), group_chans)
    summed = jnp.zeros((row_count, width), jnp.float32)
    for offset_back in range(rim_rows + 1):
        shifted = widened[rim_rows - offset_back : rim_rows - offset_back + row_count]
        summed = summed + jnp.where(window[None, :] > offset_back, shifted, jnp.float32(0.0))
    counts = jnp.minimum(window[None, :], positions[:, None] + 1).astype(jnp.float32)
    pooled = (summed / counts - widened[rim_rows:]).astype(jnp.bfloat16)
    mixed_parts = []
    for group_index in range(len(pool_windows)):
        lower = group_index * group_chans
        mixed_parts.append(
            jnp.dot(
                pooled[:, lower : lower + group_chans],
                pool_weight[group_index],
                preferred_element_type=jnp.float32,
            )
        )
    group_mix = jnp.concatenate(mixed_parts, axis=1)
    mixed_rows = rms_scale(group_mix, group_gain).astype(jnp.bfloat16)
    projected = jnp.dot(
        mixed_rows,
        lax.all_gather(out_weight, "tp", axis=1, tiled=True),
        preferred_element_type=jnp.float32,
    )
    return rms_scale(projected, out_gain).astype(jnp.bfloat16)


def expert_hidden(slot_rows, gate_local, up_local):
    gate_pre = jnp.einsum("sed,df->sef", slot_rows, gate_local, preferred_element_type=jnp.float32)
    up_pre = jnp.einsum("sed,df->sef", slot_rows, up_local, preferred_element_type=jnp.float32)
    gate_pre = jnp.minimum(gate_pre, clamp_limit)
    up_pre = jnp.clip(up_pre, -clamp_limit, clamp_limit)
    return ((up_pre + 1.0) * gate_pre * jax.nn.sigmoid(sigmoid_slope * gate_pre)).astype(
        jnp.bfloat16
    )


def send_home(hidden, down_local):
    partial_sum = jnp.einsum("sef,fd->sed", hidden, down_local, preferred_element_type=jnp.float32)
    partial_sum = partial_sum.astype(jnp.bfloat16).astype(jnp.float32)
    summed = lax.psum_scatter(
        partial_sum.astype(jnp.bfloat16), "tp", scatter_dimension=2, tiled=True
    )
    return lax.all_to_all(summed, "ep", split_axis=1, concat_axis=1, tiled=True)


def per_device(
    branch_in,
    pool_weight,
    group_gain,
    out_weight,
    out_gain,
    ffn_input,
    ffn_gain,
    routes,
    route_weight,
    gate_weight,
    up_weight,
    down_weight,
):
    mixer_out = pool_branch(branch_in, pool_weight, group_gain, out_weight, out_gain)
    normed_rows = rms_scale(ffn_input.astype(jnp.float32), ffn_gain).astype(jnp.bfloat16)
    row_count, model_width = normed_rows.shape
    top_count = routes.shape[1]
    expert_count = lax.axis_size("ep")
    capacity = 2 * row_count * top_count // expert_count
    flat_slots, owner_rows = slot_tables(routes, expert_count, capacity)
    padded = jnp.concatenate([normed_rows, jnp.zeros((1, model_width), jnp.bfloat16)], axis=0)
    slot_rows = padded[owner_rows].reshape(capacity, expert_count, model_width)
    gate_local = gate_weight[0]
    up_local = up_weight[0]
    down_local = down_weight[0]
    share = capacity // lax.axis_size("tp")
    my_share = lax.dynamic_slice_in_dim(slot_rows, lax.axis_index("tp") * share, share, 0)
    arrived = lax.all_to_all(my_share, "ep", split_axis=1, concat_axis=1, tiled=True)
    hidden = expert_hidden(lax.all_gather(arrived, "tp", axis=0, tiled=True), gate_local, up_local)
    returned = send_home(hidden, down_local)
    column_count = returned.shape[2]
    picked = returned.reshape(capacity * expert_count, column_count)[flat_slots]
    picked = picked.reshape(row_count, top_count, column_count).astype(jnp.float32)
    expert_out = jnp.sum(picked * route_weight[:, :, None], axis=1).astype(jnp.bfloat16)
    return (mixer_out, expert_out)


def solution(mesh):
    in_specs = (
        P(("ep", "tp"), None),
        P(),
        P(),
        P(None, "tp"),
        P(),
        P("ep", None),
        P(),
        P("ep", None),
        P("ep", None),
        P("ep", None, "tp"),
        P("ep", None, "tp"),
        P("ep", "tp", None),
    )
    out_specs = (P(("ep", "tp"), None), P("ep", "tp"))
    return jax.shard_map(
        per_device, mesh=mesh, in_specs=in_specs, out_specs=out_specs, check_vma=False
    )
```

profile of v0, /device:TPU:0, one launch (start us, length us, event | category | flops | bytes accessed | tf_op | source)
XLA Modules:
  0.0 230.9 jit_solution(12385050998380482686)
XLA Ops:
  7.2 0.8 copy.16
  8.4 1.1 reduce-window.6
  9.5 0.2 slice_reduce_fusion
  9.9 2.4 %scatter_custom_fusion = s32[1024]{0:T(1024)S(1)} fusion(s32[512]{0:T(512)S(1)} %bitcast.66, s32[512]{0:T(512)S(1)} %add_select_fusion, s32[]{:T(128)} %constant.34.clone.1), kind=kCustom, calls=%fused_computation.109 | custom fusion | bytes 4100 | tf_op jit(solution)/shard_map/scatter | solution.py:33
  12.3 1.2 fusion.11
  13.6 1.2 fusion.13
  14.9 6.0 %gather_fusion = bf16[1024,2048]{1,0:T(8,128)(2,1)} fusion(bf16[129,2048]{1,0:T(8,128)(2,1)S(1)} %concatenate.11, s32[1024]{0:T(1024)S(1)} %fusion.54), kind=kCustom, calls=%fused_computation | custom fusion | bytes 8392704 | tf_op jit(solution)/shard_map/gather | solution.py:114
  20.9 1.3 constant_dynamic-slice_fusion
  22.2 0.6 copy.22
  22.8 32.8 %all_to_all.10 = bf16[32,8,2048]{2,0,1:T(8,128)(2,1)} all-to-all(bf16[32,8,2048]{2,0,1:T(8,128)(2,1)S(1)} %copy.22), channel_id=1, replica_groups=mesh['ep'=8,'tp'=4] {'ep'}, dimensions={1} | all-to-all | bytes 2097152 | tf_op jit(solution)/shard_map/all_to_all | solution.py:120
  55.7 51.6 %all-gather.5.cloned.1.call-done = bf16[128,8,2048]{2,0,1:T(8,128)(2,1)} async-done(((bf16[32,8,2048]{2,0,1:T(8,128)(2,1)}), bf16[128,8,2048]{2,0,1:T(8,128)(2,1)}) %all-gather.5.cloned.1.call-update) | async-done | bytes 4194320 | tf_op jit(solution)/shard_map/all_gather | solution.py:121
  107.3 7.6 %fusion.2 = f32[128,8,1024]{2,0,1:T(8,128)S(1)} fusion(bf16[128,8,2048]{2,0,1:T(8,128)(2,1)} %all-gather.5.cloned.1.call-done, bf16[1,2048,1024]{2,1,0:T(8,128)(2,1)} %param.22), kind=kOutput, calls=%fused_computation.5 | convolution fusion | flops 4294967296 | bytes 12582912 | tf_op jit(solution)/shard_map/sed,df->sef/dot_general | solution.py:74
  115.0 5.7 %multiply_convert_fusion = bf16[128,8,1024]{2,0,1:T(8,128)(2,1)S(1)} fusion(f32[128,8,1024]{2,0,1:T(8,128)S(1)} %fusion.2, bf16[128,8,2048]{2,0,1:T(8,128)(2,1)S(1)} %copy-done.8, bf16[1,2048,1024]{2,1,0:T(8,128)(2,1)S(1)} %copy-done.6), kind=kOutput, calls=%fused_computation.9 | convolution fusion | flops 4305453056 | bytes 14680064 | tf_op jit(solution)/shard_map/sed,df->sef/dot_general | solution.py:75
  120.6 6.1 %fusion.6 = bf16[128,8,2048]{2,0,1:T(8,128)(2,1)} fusion(bf16[128,8,1024]{2,0,1:T(8,128)(2,1)S(1)} %multiply_convert_fusion, bf16[1,1024,2048]{2,1,0:T(8,128)(2,1)S(1)} %copy-done.7), kind=kOutput, calls=%fused_computation.10 | convolution fusion | flops 4297064448 | bytes 10485760 | tf_op jit(solution)/shard_map/sef,fd->sed/dot_general | solution.py:84
  126.8 0.7 all-gather.3.cloned.1.call-update
  127.5 0.2 copy-done
  127.7 3.4 %collective-permute-start = (bf16[15,512]{1,0:T(8,128)(2,1)S(1)}, bf16[15,512]{1,0:T(8,128)(2,1)S(1)}, u32[]{:S(2)}, u32[]{:S(2)}) collective-permute-start(bf16[15,512]{1,0:T(8,128)(2,1)S(1)} %slice.82), channel_id=1, source_target_pairs={{0,1},{1,2},{2,3},{3,4},{4,5},{5,6},{6,7},{7,8},{8,9},{9,10},{10,1... | collective-permute-start | bytes 46088 | tf_op jit(solution)/shard_map/ppermute | solution.py:16
  131.4 1.1 collective-permute-done
  132.6 1.1 fusion.31
  133.8 0.2 fusion.35
  134.0 45.5 %reduce-scatter.2.cloned.1.call-done = bf16[128,8,512]{2,0,1:T(8,128)(2,1)} async-done(((bf16[128,8,2048]{2,0,1:T(8,128)(2,1)}), bf16[128,8,512]{2,0,1:T(8,128)(2,1)}) %reduce-scatter.2.cloned.1.call-update) | async-done | bytes 1048592 | tf_op jit(solution)/shard_map/reduce_scatter | solution.py:86
  179.5 4.6 %all-to-all-start.1 = ((bf16[128,8,512]{2,0,1:T(8,128)(2,1)}), bf16[128,8,512]{2,0,1:T(8,128)(2,1)S(1)}, u32[]{:S(2)}, u32[]{:S(2)}) async-start(bf16[128,8,512]{2,0,1:T(8,128)(2,1)} %reduce-scatter.2.cloned.1.call-done), calls=%async_computation.2 | async-start | bytes 2097152 | tf_op jit(solution)/shard_map/all_to_all | solution.py:89
  184.1 0.2 fusion.37
  184.3 0.2 fusion.39
  184.5 0.2 fusion.41
  184.8 31.5 %all-gather.3.cloned.1.call-done = bf16[512,2048]{1,0:T(8,128)(2,1)} async-done(((bf16[512,512]{1,0:T(8,128)(2,1)}), bf16[512,2048]{1,0:T(8,128)(2,1)}) %all-gather.3.cloned.1.call-update) | async-done | bytes 2097168 | tf_op jit(solution)/shard_map/all_gather | solution.py:67
  216.4 2.5 %multiply_reduce_fusion = (f32[256]{0:T(256)S(1)}, f32[256,2048]{1,0:T(8,128)S(1)}) fusion(bf16[512,2048]{1,0:T(8,128)(2,1)} %all-gather.3.cloned.1.call-done, f32[256,128]{0,1:T(8,128)S(1)} %fusion.35, f32[256,128]{0,1:T(8,128)S(1)} %fusion.37, f32[256,128]{0,1:T(8,128)S(1)} %fusion.39, f32[256,128]{0,1:T(8,128)S(1)} %fusion.41, f32[512]{0:T(512)S(1)} %copy-done.3, ...), kind=kOutput, calls=%fused_computation.12 | convolution fusion | flops 538705664 | bytes 4722688 | tf_op jit(solution)/shard_map/dot_general | solution.py:65
  218.9 1.2 multiply_convert_fusion.1
  220.2 0.6 copy.24
  220.7 2.0 gather_fusion.1
  222.7 0.3 reshape.212
  223.0 1.4 multiply_reduce_fusion.1
  (46 shorter events, 1.2 us)
Async XLA Ops:
  7.2 100.1 %all-gather.5.cloned.1.call-start = ((), (), s32[]{:S(2)}) async-start(), calls=%async_computation.4 | async-start | bytes 5242880 | tf_op jit(solution)/shard_map/all_gather | solution.py:121
  55.6 123.9 %reduce-scatter.2.cloned.1.call-start = ((), (), s32[]{:S(2)}) async-start(), calls=%async_computation.5 | async-start | bytes 5242880 | tf_op jit(solution)/shard_map/reduce_scatter | solution.py:86
  107.3 7.7 %copy-start.6 = (bf16[1,2048,1024]{2,1,0:T(8,128)(2,1)S(1)}, bf16[1,2048,1024]{2,1,0:T(8,128)(2,1)}, u32[]{:S(2)}) copy-start(bf16[1,2048,1024]{2,1,0:T(8,128)(2,1)} %param.23) | copy-start | bytes 12582916
  107.3 7.7 %copy-start.8 = (bf16[128,8,2048]{2,0,1:T(8,128)(2,1)S(1)}, bf16[128,8,2048]{2,0,1:T(8,128)(2,1)}, u32[]{:S(2)}) copy-start(bf16[128,8,2048]{2,0,1:T(8,128)(2,1)} %all-gather.5.cloned.1.call-done) | copy-start | bytes 12582916
  115.0 5.7 %copy-start.7 = (bf16[1,1024,2048]{2,1,0:T(8,128)(2,1)S(1)}, bf16[1,1024,2048]{2,1,0:T(8,128)(2,1)}, u32[]{:S(2)}) copy-start(bf16[1,1024,2048]{2,1,0:T(8,128)(2,1)} %param.24) | copy-start | bytes 12582916
  126.7 0.9 copy-start
  126.7 4.4 %copy-start.5 = (s32[4]{0:T(128)S(1)}, s32[4]{0:T(128)}, u32[]{:S(2)}) copy-start(s32[4]{0:T(128)} %constant.101.clone) | copy-start | bytes 52
  126.7 4.5 %copy-start.4 = (f32[128,4]{0,1:T(4,128)S(1)}, f32[128,4]{0,1:T(4,128)}, u32[]{:S(2)}) copy-start(f32[128,4]{0,1:T(4,128)} %param.21) | copy-start | bytes 6148
  126.7 89.6 %all-gather.3.cloned.1.call-start = ((), (), s32[]{:S(2)}) async-start(), calls=%async_computation.3 | async-start | bytes 2621440 | tf_op jit(solution)/shard_map/all_gather | solution.py:67
  127.7 4.8 %collective-permute-start = (bf16[15,512]{1,0:T(8,128)(2,1)S(1)}, bf16[15,512]{1,0:T(8,128)(2,1)S(1)}, u32[]{:S(2)}, u32[]{:S(2)}) collective-permute-start(bf16[15,512]{1,0:T(8,128)(2,1)S(1)} %slice.82), channel_id=1, source_target_pairs={{0,1},{1,2},{2,3},{3,4},{4,5},{5,6},{6,7},{7,8},{8,9},{9,10},{10,1... | collective-permute-start | bytes 46088 | tf_op jit(solution)/shard_map/ppermute | solution.py:16
  132.6 1.2 copy-start.1
  132.6 83.8 %copy-start.3 = (f32[512]{0:T(512)S(1)}, f32[512]{0:T(512)}, u32[]{:S(2)}) copy-start(f32[512]{0:T(512)} %param.15) | copy-start | bytes 6148
  133.7 85.2 %copy-start.2 = (f32[2048]{0:T(1024)S(1)}, f32[2048]{0:T(1024)}, u32[]{:S(2)}) copy-start(f32[2048]{0:T(1024)} %param.17) | copy-start | bytes 24580
  179.5 40.7 %all-to-all-start.1 = ((bf16[128,8,512]{2,0,1:T(8,128)(2,1)}), bf16[128,8,512]{2,0,1:T(8,128)(2,1)S(1)}, u32[]{:S(2)}, u32[]{:S(2)}) async-start(bf16[128,8,512]{2,0,1:T(8,128)(2,1)} %reduce-scatter.2.cloned.1.call-done), calls=%async_computation.2 | async-start | bytes 2097152 | tf_op jit(solution)/shard_map/all_to_all | solution.py:89
Sparse Core Ops, SparseCore 0:
  55.7 51.4 all-gather.4
  126.9 52.5 reduce-scatter.1
  181.3 35.0 all-gather.2
where the time goes:
time: 231 us
  waiting for transfers between devices  130 us (56%)
  blocking collectives  32.8 us (14%)
  matrix products  22.7 us (10%)
  local copies, waits for them, and re-layouts  15 us (6%)
  between operations  14 us (6%)
  starting transfers between devices  8.11 us (4%)
  other arithmetic  7.78 us (3%)
    all_gather x1, waiting for transfers between devices, per_device(): lax.all_gather(arrived, 'tp', axis=0, tiled=True)  51.6 us
    reduce_scatter x1, waiting for transfers between devices, send_home(): lax.psum_scatter(partial_sum.astype(jnp.bfloat16), 'tp', scatter_dimensio...  45.5 us
    all_to_all x1, blocking collectives, per_device(): lax.all_to_all(my_share, 'ep', split_axis=1, concat_axis=1, tiled=True)  32.8 us
    all_gather x1, waiting for transfers between devices, pool_branch(): lax.all_gather(out_weight, 'tp', axis=1, tiled=True)  31.5 us
    dot_general x1, matrix products, expert_hidden(): jnp.einsum('sed,df->sef', slot_rows, gate_local, preferred_element_type=j...  7.64 us
    dot_general x1, matrix products, send_home(): jnp.einsum('sef,fd->sed', hidden, down_local, preferred_element_type=jnp....  6.07 us
    gather x1, local copies, waits for them, and re-layouts, per_device(): slot_rows = padded[owner_rows].reshape(capacity, expert_count, model_width)  6.02 us
    dot_general x1, matrix products, expert_hidden(): jnp.einsum('sed,df->sef', slot_rows, up_local, preferred_element_type=jnp...  5.65 us
  transfers between devices with their start and end apart: 5, of which 4 were waited for; matrix products, arithmetic and copies ran while one was open for 3% of the time, Pallas kernels for 0%

commit v1 on v0

--- a/solution.py
+++ b/solution.py
@@ -8,6 +8,18 @@
 norm_eps = 1e-06
 clamp_limit = 7.0
 sigmoid_slope = 1.702
+
+
+def gather_by_bits(x, axis, dim):
+    ways, here = (lax.axis_size(axis), lax.axis_index(axis))
+    grown, reach = (x, 1)
+    while reach < ways:
+        theirs = lax.ppermute(grown, axis, [(d, d ^ reach) for d in range(ways)])
+        mine_first = jnp.concatenate([grown, theirs], axis=dim)
+        theirs_first = jnp.concatenate([theirs, grown], axis=dim)
+        grown = jnp.where(here & reach == 0, mine_first, theirs_first)
+        reach = 2 * reach
+    return grown
 
 
 def shifted_2(block, axis, distance):
@@ -118,7 +130,7 @@
     share = capacity // lax.axis_size("tp")
     my_share = lax.dynamic_slice_in_dim(slot_rows, lax.axis_index("tp") * share, share, 0)
     arrived = lax.all_to_all(my_share, "ep", split_axis=1, concat_axis=1, tiled=True)
-    hidden = expert_hidden(lax.all_gather(arrived, "tp", axis=0, tiled=True), gate_local, up_local)
+    hidden = expert_hidden(gather_by_bits(arrived, "tp", 0), gate_local, up_local)
     returned = send_home(hidden, down_local)
     column_count = returned.shape[2]
     picked = returned.reshape(capacity * expert_count, column_count)[flat_slots]

time: 231 us -> 260 us (1.13)
  waiting for transfers between devices: 130 us -> 147 us
  matrix products: 22.7 us -> 29.7 us
  starting transfers between devices: 8.11 us -> 11.3 us
    ppermute x0 -> x2, waiting for transfers between devices: none -> 67.9 us  [gather_by_bits(): theirs = lax.ppermute(grown, axis, [(d, d ^ reach) for d in range(ways)])]
    all_gather x1 -> x0, waiting for transfers between devices: 51.6 us -> none  [per_device(): lax.all_gather(arrived, 'tp', axis=0, tiled=True)]
    dot_general x1, matrix products: 6.07 us -> 16.5 us  [send_home(): jnp.einsum('sef,fd->sed', hidden, down_local, preferred_element_type=jnp....]
    dot_general x1 -> x0, matrix products: 7.64 us -> none  [expert_hidden(): jnp.einsum('sed,df->sef', slot_rows, gate_local, preferred_element_type=j...]
    dot_general x1, matrix products: 5.65 us -> 9.94 us  [expert_hidden(): jnp.einsum('sed,df->sef', slot_rows, up_local, preferred_element_type=jnp...]
    ppermute x0 -> x2, starting transfers between devices: none -> 3.08 us  [gather_by_bits(): theirs = lax.ppermute(grown, axis, [(d, d ^ reach) for d in range(ways)])]
  transfers between devices with their start and end apart: 5 -> 6, of which waited for: 4 -> 5; matrix products, arithmetic and copies ran while one was open for 3% -> 2% of each run, Pallas kernels for 0% -> 0%
where the time goes in v1:
time: 260 us
  waiting for transfers between devices  147 us (57%)
  blocking collectives  32.7 us (13%)
  matrix products  29.7 us (11%)
  local copies, waits for them, and re-layouts  15 us (6%)
  between operations  14.3 us (6%)
  starting transfers between devices  11.3 us (4%)
  other arithmetic  10.2 us (4%)
    ppermute x2, waiting for transfers between devices, gather_by_bits(): theirs = lax.ppermute(grown, axis, [(d, d ^ reach) for d in range(ways)])  67.9 us
    reduce_scatter x1, waiting for transfers between devices, send_home(): lax.psum_scatter(partial_sum.astype(jnp.bfloat16), 'tp', scatter_dimensio...  45.7 us
    all_to_all x1, blocking collectives, per_device(): lax.all_to_all(my_share, 'ep', split_axis=1, concat_axis=1, tiled=True)  32.7 us
    all_gather x1, waiting for transfers between devices, pool_branch(): lax.all_gather(out_weight, 'tp', axis=1, tiled=True)  31.6 us
    dot_general x1, matrix products, send_home(): jnp.einsum('sef,fd->sed', hidden, down_local, preferred_element_type=jnp....  16.5 us
    dot_general x1, matrix products, expert_hidden(): jnp.einsum('sed,df->sef', slot_rows, up_local, preferred_element_type=jnp...  9.94 us
    gather x1, local copies, waits for them, and re-layouts, per_device(): slot_rows = padded[owner_rows].reshape(capacity, expert_count, model_width)  6.02 us
  transfers between devices with their start and end apart: 6, of which 5 were waited for; matrix products, arithmetic and copies ran while one was open for 2% of the time, Pallas kernels for 0%

profile of v1, /device:TPU:0, one launch (start us, length us, event | category | flops | bytes accessed | tf_op | source)
XLA Modules:
  0.0 259.9 jit_solution(3403495987471954472)
XLA Ops:
  7.2 0.8 copy.17
  8.4 1.1 reduce-window.6
  9.5 0.2 slice_reduce_fusion
  9.9 2.4 scatter_custom_fusion
  12.3 1.2 fusion.11
  13.6 1.2 fusion.13
  14.9 6.0 %gather_fusion = bf16[1024,2048]{1,0:T(8,128)(2,1)} fusion(bf16[129,2048]{1,0:T(8,128)(2,1)S(1)} %concatenate.23, s32[1024]{0:T(1024)S(1)} %fusion.56), kind=kCustom, calls=%fused_computation | custom fusion | bytes 8392704 | tf_op jit(solution)/shard_map/gather | solution.py:126
  20.9 1.3 constant_dynamic-slice_fusion
  22.2 0.6 copy.23
  22.8 32.7 %all_to_all.10 = bf16[32,8,2048]{2,0,1:T(8,128)(2,1)S(1)} all-to-all(bf16[32,8,2048]{2,0,1:T(8,128)(2,1)S(1)} %copy.23), channel_id=1, replica_groups=mesh['ep'=8,'tp'=4] {'ep'}, dimensions={1} | all-to-all | bytes 2097152 | tf_op jit(solution)/shard_map/all_to_all | solution.py:132
  55.5 1.5 collective-permute-start.1
  57.0 23.1 %collective-permute-done.1 = bf16[32,8,2048]{2,0,1:T(8,128)(2,1)} collective-permute-done((bf16[32,8,2048]{2,0,1:T(8,128)(2,1)S(1)}, bf16[32,8,2048]{2,0,1:T(8,128)(2,1)}, u32[]{:S(2)}, u32[]{:S(2)}) %collective-permute-start.1) | collective-permute-done | bytes 1048608 | tf_op jit(solution)/shard_map/ppermute | solution.py:17
  80.1 2.4 maximum_select_fusion.1
  82.5 1.6 collective-permute-start.2
  84.1 44.7 %collective-permute-done.2 = bf16[64,8,2048]{2,0,1:T(8,128)(2,1)} collective-permute-done((bf16[64,8,2048]{2,0,1:T(8,128)(2,1)S(1)}, bf16[64,8,2048]{2,0,1:T(8,128)(2,1)}, u32[]{:S(2)}, u32[]{:S(2)}) %collective-permute-start.2) | collective-permute-done | bytes 2097184 | tf_op jit(solution)/shard_map/ppermute | solution.py:17
  128.8 9.9 %fusion.4 = f32[128,8,1024]{2,0,1:T(8,128)} fusion(bf16[1,2048,1024]{2,1,0:T(8,128)(2,1)} %param.23, bf16[64,8,2048]{2,0,1:T(8,128)(2,1)} %collective-permute-done.2, bf16[64,8,2048]{2,0,1:T(8,128)(2,1)S(1)} %maximum_select_fusion.1, pred[]{:T(512)S(6)} %eq.31), kind=kOutput, calls=%fused_computation.8 | convolution fusion | flops 4313841664 | bytes 12582913 | tf_op jit(solution)/shard_map/sed,df->sef/dot_general | solution.py:87
  138.8 16.5 %fusion.6 = bf16[128,8,2048]{2,0,1:T(8,128)(2,1)} fusion(bf16[1,1024,2048]{2,1,0:T(8,128)(2,1)} %param.24, f32[128,8,1024]{2,0,1:T(8,128)} %fusion.4, bf16[1,2048,1024]{2,1,0:T(8,128)(2,1)} %param.22, bf16[64,8,2048]{2,0,1:T(8,128)(2,1)} %collective-permute-done.2, bf16[64,8,2048]{2,0,1:T(8,128)(2,1)S(1)} %maximum_select_fusion.1, pred[]{:T(512)S(6)} %eq.31), kind=kOutput, calls=%fused_computation.11 | convolution fusion | flops 8621391872 | bytes 20971520 | tf_op jit(solution)/shard_map/sef,fd->sed/dot_general | solution.py:96
  155.3 0.7 all-gather.2.cloned.1.call-update
  156.2 3.6 %collective-permute-start = (bf16[15,512]{1,0:T(8,128)(2,1)S(1)}, bf16[15,512]{1,0:T(8,128)(2,1)S(1)}, u32[]{:S(2)}, u32[]{:S(2)}) collective-permute-start(bf16[15,512]{1,0:T(8,128)(2,1)S(1)} %slice.82), channel_id=1, source_target_pairs={{0,1},{1,2},{2,3},{3,4},{4,5},{5,6},{6,7},{7,8},{8,9},{9,10},{10,1... | collective-permute-start | bytes 46088 | tf_op jit(solution)/shard_map/ppermute | solution.py:28
  160.1 0.9 collective-permute-done
  161.1 1.1 fusion.33
  162.3 0.2 fusion.37
  162.5 45.7 %reduce-scatter.2.cloned.1.call-done = bf16[128,8,512]{2,0,1:T(8,128)(2,1)} async-done(((bf16[128,8,2048]{2,0,1:T(8,128)(2,1)}), bf16[128,8,512]{2,0,1:T(8,128)(2,1)}) %reduce-scatter.2.cloned.1.call-update) | async-done | bytes 1048592 | tf_op jit(solution)/shard_map/reduce_scatter | solution.py:98
  208.2 4.6 %all-to-all-start.1 = ((bf16[128,8,512]{2,0,1:T(8,128)(2,1)}), bf16[128,8,512]{2,0,1:T(8,128)(2,1)S(1)}, u32[]{:S(2)}, u32[]{:S(2)}) async-start(bf16[128,8,512]{2,0,1:T(8,128)(2,1)} %reduce-scatter.2.cloned.1.call-done), calls=%async_computation.2 | async-start | bytes 2097152 | tf_op jit(solution)/shard_map/all_to_all | solution.py:101
  213.2 0.2 fusion.43
  213.5 31.6 %all-gather.2.cloned.1.call-done = bf16[512,2048]{1,0:T(8,128)(2,1)} async-done(((bf16[512,512]{1,0:T(8,128)(2,1)}), bf16[512,2048]{1,0:T(8,128)(2,1)}) %all-gather.2.cloned.1.call-update) | async-done | bytes 2097168 | tf_op jit(solution)/shard_map/all_gather | solution.py:79
  245.1 2.5 multiply_reduce_fusion
  247.6 1.2 multiply_convert_fusion.1
  248.8 0.6 copy.25
  249.4 2.0 gather_fusion.1
  251.4 0.3 reshape.212
  251.7 1.4 multiply_reduce_fusion.1
  (41 shorter events, 1.7 us)
Async XLA Ops:
  7.2 201.0 %reduce-scatter.2.cloned.1.call-start = ((), (), s32[]{:S(2)}) async-start(), calls=%async_computation.4 | async-start | bytes 5242880 | tf_op jit(solution)/shard_map/reduce_scatter | solution.py:98
  55.5 24.6 %collective-permute-start.1 = (bf16[32,8,2048]{2,0,1:T(8,128)(2,1)S(1)}, bf16[32,8,2048]{2,0,1:T(8,128)(2,1)}, u32[]{:S(2)}, u32[]{:S(2)}) collective-permute-start(bf16[32,8,2048]{2,0,1:T(8,128)(2,1)S(1)} %all_to_all.10), channel_id=1, source_target_pairs={{0,1},{1,0},{2,3},{3,2},{4,5},{5,4},{6,7},{7,6},{8,9},{9,8},{10,11... | collective-permute-start | bytes 3145736 | tf_op jit(solution)/shard_map/ppermute | solution.py:17
  82.5 46.3 %collective-permute-start.2 = (bf16[64,8,2048]{2,0,1:T(8,128)(2,1)S(1)}, bf16[64,8,2048]{2,0,1:T(8,128)(2,1)}, u32[]{:S(2)}, u32[]{:S(2)}) collective-permute-start(bf16[64,8,2048]{2,0,1:T(8,128)(2,1)S(1)} %maximum_select_fusion.1), channel_id=1, source_target_pairs={{0,2},{1,3},{2,0},{3,1},{4,6},{5,7},{6,4},{7,5},{8,10},{9,11},{10,... | collective-permute-start | bytes 6291464 | tf_op jit(solution)/shard_map/ppermute | solution.py:17
  155.2 0.9 copy-start
  155.2 4.6 %copy-start.5 = (s32[4]{0:T(128)S(1)}, s32[4]{0:T(128)}, u32[]{:S(2)}) copy-start(s32[4]{0:T(128)} %constant.103.clone) | copy-start | bytes 52
  155.2 4.7 %copy-start.4 = (f32[128,4]{0,1:T(4,128)S(1)}, f32[128,4]{0,1:T(4,128)}, u32[]{:S(2)}) copy-start(f32[128,4]{0,1:T(4,128)} %param.21) | copy-start | bytes 6148
  155.3 89.8 %all-gather.2.cloned.1.call-start = ((), (), s32[]{:S(2)}) async-start(), calls=%async_computation.3 | async-start | bytes 2621440 | tf_op jit(solution)/shard_map/all_gather | solution.py:79
  156.2 4.8 %collective-permute-start = (bf16[15,512]{1,0:T(8,128)(2,1)S(1)}, bf16[15,512]{1,0:T(8,128)(2,1)S(1)}, u32[]{:S(2)}, u32[]{:S(2)}) collective-permute-start(bf16[15,512]{1,0:T(8,128)(2,1)S(1)} %slice.82), channel_id=1, source_target_pairs={{0,1},{1,2},{2,3},{3,4},{4,5},{5,6},{6,7},{7,8},{8,9},{9,10},{10,1... | collective-permute-start | bytes 46088 | tf_op jit(solution)/shard_map/ppermute | solution.py:28
  161.1 1.2 copy-start.1
  161.1 84.0 %copy-start.3 = (f32[512]{0:T(512)S(1)}, f32[512]{0:T(512)}, u32[]{:S(2)}) copy-start(f32[512]{0:T(512)} %param.15) | copy-start | bytes 6148
  162.3 85.3 %copy-start.2 = (f32[2048]{0:T(1024)S(1)}, f32[2048]{0:T(1024)}, u32[]{:S(2)}) copy-start(f32[2048]{0:T(1024)} %param.17) | copy-start | bytes 24580
  208.2 40.6 %all-to-all-start.1 = ((bf16[128,8,512]{2,0,1:T(8,128)(2,1)}), bf16[128,8,512]{2,0,1:T(8,128)(2,1)S(1)}, u32[]{:S(2)}, u32[]{:S(2)}) async-start(bf16[128,8,512]{2,0,1:T(8,128)(2,1)} %reduce-scatter.2.cloned.1.call-done), calls=%async_computation.2 | async-start | bytes 2097152 | tf_op jit(solution)/shard_map/all_to_all | solution.py:101
Sparse Core Ops, SparseCore 0:
  155.4 52.7 reduce-scatter.1
  210.0 35.0 all-gather.1
